TPU v7x, 32 devices: a whole 2x2x4 slice. The times are simulated.
32 devices in a mesh: rep: 2 (over x), fs: 4 (over z), tp: 4 (over y, core).
Axes of the slice: x: 2, y: 2, z: 4, core: 2. Of those that a mesh axis runs over, the one named last changes fastest.
Arguments:
- tokens: bfloat16 [8, 1024, 2048], P(('rep', 'fs')), may hold values from -6 to 6
- mix_gain: bfloat16 [2048], replicated, may hold values from 0.099609375 to 1.8984375
- value_weight: bfloat16 [2048, 1024], P('fs', 'tp'), may hold values from -0.125 to 0.125
- gate_weight: bfloat16 [2048, 1024], P('fs', 'tp'), may hold values from -0.125 to 0.125
- mix_taps: bfloat16 [31, 1024], P(None, 'tp'), may hold values from -1 to 1
- head_gain: bfloat16 [1024], P('tp'), may hold values from 0.099609375 to 1.8984375
- out_weight: bfloat16 [1024, 2048], P('fs', 'tp'), may hold values from -0.1875 to 0.1875
- ffn_gain: bfloat16 [2048], replicated, may hold values from 0.099609375 to 1.8984375
- ffgate_weight: bfloat16 [2048, 6144], P('fs', 'tp'), may hold values from -0.125 to 0.125
- up_weight: bfloat16 [2048, 6144], P('fs', 'tp'), may hold values from -0.125 to 0.125
- ff_taps: bfloat16 [3, 6144], P(None, 'tp'), may hold values from -3.5 to 3.5
- down_weight: bfloat16 [2048, 6144], P('fs', 'tp'), may hold values from -0.078125 to 0.078125
Outputs:
- layer_out: bfloat16 [8, 1024, 2048], P(('rep', 'fs'), 'tp')
All inputs are finite; a program needn't handle non-finite values.
Results may differ from a plain program's by a relative error of at most 0.01.
Values may be sent and summed in bfloat16 or wider, within the bound.
No kernel may reach another device: no remote copies, remote signals or barrier semaphores. Data moves between devices by JAX's collectives and lax.ppermute only.
A program may use at most 128 MiB of HBM per device.

v0:
```python
import jax
import jax.numpy as jnp
from jax import lax
from jax.sharding import PartitionSpec as P

HEAD = 128
norm_floor = 0.01


def row_norm(floats_in, scales):
    floats = floats_in.astype(jnp.float32)
    scaled = floats * lax.rsqrt(jnp.mean(floats * floats, axis=-1, keepdims=True) + norm_floor)
    return (scaled * scales.astype(jnp.float32)).astype(jnp.bfloat16)


def causal_conv(signal, kernel_taps):
    reach = kernel_taps.shape[0]
    length = signal.shape[0]
    padded = jnp.pad(signal, ((reach - 1, 0), (0, 0)))
    summed = padded[0:length] * kernel_taps[0]
    for offset in range(1, reach):
        summed = summed + padded[offset : offset + length] * kernel_taps[offset]
    return summed


def head_norm(signal, scales):
    length = signal.shape[0]
    grouped = signal.reshape(length, signal.shape[1] // HEAD, HEAD)
    centre = grouped - jnp.mean(grouped, axis=-1, keepdims=True)
    spread = jnp.mean(centre * centre, axis=-1, keepdims=True)
    normal = (centre * lax.rsqrt(spread + norm_floor)).reshape(signal.shape)
    return normal * scales.astype(jnp.float32)


def on_device(
    tokens,
    mix_gain,
    value_weight,
    gate_weight,
    mix_taps,
    head_gain,
    out_weight,
    ffn_gain,
    ffgate_weight,
    up_weight,
    ff_taps,
    down_weight,
):
    sequence = tokens[0]
    value_full, gate_full, out_full = (
        lax.all_gather(value_weight, "fs", axis=0, tiled=True),
        lax.all_gather(gate_weight, "fs", axis=0, tiled=True),
        lax.all_gather(out_weight, "fs", axis=0, tiled=True),
    )
    normed = row_norm(sequence, mix_gain)
    values = jnp.dot(normed, value_full, preferred_element_type=jnp.float32)
    gating = jnp.dot(normed, gate_full, preferred_element_type=jnp.float32)
    glu_out = values * jax.nn.sigmoid(gating)
    mixed_pos = causal_conv(glu_out, mix_taps.astype(jnp.float32))
    head_out = jax.nn.silu(head_norm(mixed_pos, head_gain)).astype(jnp.bfloat16)
    out_cols = out_full.shape[1]
    mixer_sum = jnp.dot(
        lax.all_gather(head_out, "tp", axis=1, tiled=True),
        out_full,
        preferred_element_type=jnp.float32,
    )
    own_cols = lax.dynamic_slice_in_dim(sequence, lax.axis_index("tp") * out_cols, out_cols, 1)
    hidden_cols = (own_cols.astype(jnp.float32) + mixer_sum).astype(jnp.bfloat16)
    full_rows = lax.all_gather(hidden_cols, "tp", axis=1, tiled=True)
    normed_ffn = row_norm(full_rows, ffn_gain)
    block_rows = normed_ffn
    ffgate = jnp.dot(
        block_rows,
        lax.all_gather(ffgate_weight, "fs", axis=0, tiled=True),
        preferred_element_type=jnp.float32,
    )
    ff_up = jnp.dot(
        block_rows,
        lax.all_gather(up_weight, "fs", axis=0, tiled=True),
        preferred_element_type=jnp.float32,
    )
    down_full = lax.all_gather(down_weight, "fs", axis=0, tiled=True)
    product = (jax.nn.silu(causal_conv(ffgate, ff_taps.astype(jnp.float32))) * ff_up).astype(
        jnp.bfloat16
    )
    own_count = sequence.shape[0] // lax.axis_size("tp")
    block_rows = product
    summed_rows = lax.psum_scatter(
        lax.dot_general(
            block_rows, down_full, (((1,), (1,)), ((), ())), preferred_element_type=jnp.float32
        ).astype(jnp.bfloat16),
        "tp",
        scatter_dimension=0,
        tiled=True,
    ).astype(jnp.float32)
    own_rows = lax.dynamic_slice_in_dim(full_rows, lax.axis_index("tp") * own_count, own_count, 0)
    return (own_rows.astype(jnp.float32) + summed_rows).astype(jnp.bfloat16)[None]


def solution(mesh):
    placed = (
        P(("rep", "fs"), None, None),
        P(),
        P("fs", "tp"),
        P("fs", "tp"),
        P(None, "tp"),
        P("tp"),
        P("fs", "tp"),
        P(),
        P("fs", "tp"),
        P("fs", "tp"),
        P(None, "tp"),
        P("fs", "tp"),
    )
    return jax.shard_map(
        on_device,
        mesh=mesh,
        in_specs=placed,
        out_specs=P(("rep", "fs"), "tp", None),
        check_vma=False,
    )
```

profile of v0, /device:TPU:0, one launch (start us, length us, event | category | flops | bytes accessed | tf_op | source)
XLA Modules:
  0.0 585.6 jit_solution(9061015034751386322)
XLA Ops:
  8.8 1.0 fusion.38
  9.8 1.0 fusion.39
  10.8 3.1 fusion.3
  15.2 24.4 %all-gather.11.cloned.1.call-done = bf16[2048,256]{1,0:T(8,128)(2,1)} async-done(((bf16[512,256]{1,0:T(8,128)(2,1)}), bf16[2048,256]{1,0:T(8,128)(2,1)}) %all-gather.11.cloned.1.call-update) | async-done | bytes 1048592 | tf_op jit(solution)/shard_map/all_gather | solution.py:52
  39.6 3.8 fusion.9
  43.5 25.1 %all-gather.9.cloned.1.call-done = bf16[2048,256]{1,0:T(8,128)(2,1)} async-done(((bf16[512,256]{1,0:T(8,128)(2,1)}), bf16[2048,256]{1,0:T(8,128)(2,1)}) %all-gather.9.cloned.1.call-update) | async-done | bytes 1048592 | tf_op jit(solution)/shard_map/all_gather | solution.py:51
  68.6 3.8 convolution_multiply_fusion
  72.4 4.2 multiply_add_fusion
  77.2 1.1 reduce_sum.37
  78.4 14.4 %multiply_reduce_fusion = f32[1024,2]{1,0:T(8,128)S(1)} fusion(f32[1024,2,128]{2,1,0:T(2,128)S(1)} %reshape.42, f32[1024,2]{1,0:T(8,128)S(1)} %broadcast_multiply_fusion), kind=kLoop, calls=%fused_computation.26 | loop fusion | flops 784384 | bytes 1064960 | tf_op jit(solution)/shard_map/reduce_sum | solution.py:30
  92.9 1.2 mul.521
  94.1 1.2 sub.13
  95.4 5.8 multiply_convert_fusion.1
  101.3 22.2 %all-gather.13.cloned.1.call-done = bf16[1024,1024]{1,0:T(8,128)(2,1)} async-done(((bf16[1024,256]{1,0:T(8,128)(2,1)}), bf16[1024,1024]{1,0:T(8,128)(2,1)}) %all-gather.13.cloned.1.call-update) | async-done | bytes 2097168 | tf_op jit(solution)/shard_map/all_gather | solution.py:63
  123.5 4.4 fusion.6
  130.2 32.4 %all-gather.17.cloned.1.call-done = bf16[1024,2048]{1,0:T(8,128)(2,1)} async-done(((bf16[1024,512]{1,0:T(8,128)(2,1)}), bf16[1024,2048]{1,0:T(8,128)(2,1)}) %all-gather.17.cloned.1.call-update) | async-done | bytes 4194320 | tf_op jit(solution)/shard_map/all_gather | solution.py:69
  162.6 3.1 fusion
  165.7 113.7 %all-gather.19.cloned.1.call-done = bf16[2048,1536]{1,0:T(8,128)(2,1)} async-done(((bf16[512,1536]{1,0:T(8,128)(2,1)}), bf16[2048,1536]{1,0:T(8,128)(2,1)}) %all-gather.19.cloned.1.call-update) | async-done | bytes 6291472 | tf_op jit(solution)/shard_map/all_gather | solution.py:74
  279.4 12.2 %fusion.11 = f32[1024,1536]{1,0:T(8,128)} fusion(bf16[2048,1536]{1,0:T(8,128)(2,1)} %all-gather.19.cloned.1.call-done, bf16[1024,2048]{1,0:T(8,128)(2,1)} %all-gather.17.cloned.1.call-done, f32[2048]{0:T(1024)S(1)} %convert_element_type.73, f32[1024]{0:T(1024)S(1)} %add_rsqrt_fusion.1), kind=kOutput, calls=%fused_computation.20 | convolution fusion | flops 6450839552 | bytes 16789504 | tf_op jit(solution)/shard_map/dot_general | solution.py:72
  291.5 102.9 %all-gather.21.cloned.1.call-done = bf16[2048,1536]{1,0:T(8,128)(2,1)} async-done(((bf16[512,1536]{1,0:T(8,128)(2,1)}), bf16[2048,1536]{1,0:T(8,128)(2,1)}) %all-gather.21.cloned.1.call-update) | async-done | bytes 6291472 | tf_op jit(solution)/shard_map/all_gather | solution.py:79
  394.5 115.1 %all-gather.23.cloned.1.call-done = bf16[2048,1536]{1,0:T(8,128)(2,1)} async-done(((bf16[512,1536]{1,0:T(8,128)(2,1)}), bf16[2048,1536]{1,0:T(8,128)(2,1)}) %all-gather.23.cloned.1.call-update) | async-done | bytes 6291472 | tf_op jit(solution)/shard_map/all_gather | solution.py:82
  509.6 23.6 %convolution_convert_fusion = bf16[1024,2048]{1,0:T(8,128)(2,1)} fusion(bf16[2048,1536]{1,0:T(8,128)(2,1)} %all-gather.23.cloned.1.call-done, f32[1024,1536]{1,0:T(8,128)} %fusion.11, bf16[2048,1536]{1,0:T(8,128)(2,1)} %all-gather.21.cloned.1.call-done, f32[1536]{0:T(1024)S(1)} %get-tuple-element.6, f32[1536]{0:T(1024)S(1)} %get-tuple-element.7, ...), kind=kOutput, calls=%fused_computation.11 | convolution fusion | flops 12912689152 | bytes 27293696 | tf_op jit(solution)/shard_map/dot_general | solution.py:89
  533.2 42.9 %reduce-scatter.2.cloned.1.call-done = bf16[256,2048]{1,0:T(8,128)(2,1)} async-done(((bf16[1024,2048]{1,0:T(8,128)(2,1)}), bf16[256,2048]{1,0:T(8,128)(2,1)}) %reduce-scatter.2.cloned.1.call-update) | async-done | bytes 1048592 | tf_op jit(solution)/shard_map/reduce_scatter | solution.py:88
  576.1 2.9 fusion.15
  (33 shorter events, 6.5 us)
Async XLA Ops:
  6.5 33.1 %all-gather.11.cloned.1.call-start = ((), (), s32[]{:S(2)}) async-start(), calls=%async_computation.2 | async-start | bytes 1310720 | tf_op jit(solution)/shard_map/all_gather | solution.py:52
  7.3 61.3 %all-gather.9.cloned.1.call-start = ((), (), s32[]{:S(2)}) async-start(), calls=%async_computation.1 | async-start | bytes 1310720 | tf_op jit(solution)/shard_map/all_gather | solution.py:51
  8.0 93.3 %all-gather.15.cloned.1.call-start = ((), (), s32[]{:S(2)}) async-start(), calls=%async_computation.4 | async-start | bytes 1310720 | tf_op jit(solution)/shard_map/all_gather | solution.py:53
  8.7 114.8 %all-gather.13.cloned.1.call-start = ((), (), s32[]{:S(2)}) async-start(), calls=%async_computation.3 | async-start | bytes 2621440 | tf_op jit(solution)/shard_map/all_gather | solution.py:63
  101.2 61.4 %all-gather.17.cloned.1.call-start = ((), (), s32[]{:S(2)}) async-start(), calls=%async_computation.5 | async-start | bytes 5242880 | tf_op jit(solution)/shard_map/all_gather | solution.py:69
  101.2 28.8 %copy-start.1 = (bf16[2048]{0:T(1024)(128)(2,1)S(1)}, bf16[2048]{0:T(1024)(128)(2,1)}, u32[]{:S(2)}) copy-start(bf16[2048]{0:T(1024)(128)(2,1)} %param.19) | copy-start | bytes 12292
  101.3 28.9 %copy-start = (bf16[3,1536]{1,0:T(4,128)(2,1)S(1)}, bf16[3,1536]{1,0:T(4,128)(2,1)}, u32[]{:S(2)}) copy-start(bf16[3,1536]{1,0:T(4,128)(2,1)} %param.22) | copy-start | bytes 27652
  128.0 151.4 %all-gather.19.cloned.1.call-start = ((), (), s32[]{:S(2)}) async-start(), calls=%async_computation.6 | async-start | bytes 7864320 | tf_op jit(solution)/shard_map/all_gather | solution.py:74
  128.5 265.9 %all-gather.21.cloned.1.call-start = ((), (), s32[]{:S(2)}) async-start(), calls=%async_computation.7 | async-start | bytes 7864320 | tf_op jit(solution)/shard_map/all_gather | solution.py:79
  129.3 380.3 %all-gather.23.cloned.1.call-start = ((), (), s32[]{:S(2)}) async-start(), calls=%async_computation.8 | async-start | bytes 7864320 | tf_op jit(solution)/shard_map/all_gather | solution.py:82
  130.0 446.1 %reduce-scatter.2.cloned.1.call-start = ((), (), s32[]{:S(2)}) async-start(), calls=%async_computation.9 | async-start | bytes 5242880 | tf_op jit(solution)/shard_map/reduce_scatter | solution.py:88
Sparse Core Ops, SparseCore 0:
  8.9 30.6 all-gather.10
  41.2 27.3 all-gather.8
  70.2 27.3 all-gather.14
  101.3 22.1 all-gather.12
  128.1 34.4 all-gather.16
  164.0 115.3 all-gather.18
  280.9 113.4 all-gather.20
  396.0 113.5 all-gather.22
  533.3 42.7 reduce-scatter.1
where the time goes:
time: 586 us
  waiting for transfers between devices  483 us (82%)
  matrix products  47.8 us (8%)
  other arithmetic  36.1 us (6%)
  between operations  13.4 us (2%)
    all_gather x1, waiting for transfers between devices, on_device(): down_full = lax.all_gather(down_weight, 'fs', axis=0, tiled=True)  115 us
    all_gather x1, waiting for transfers between devices, on_device(): lax.all_gather(ffgate_weight, 'fs', axis=0, tiled=True)  114 us
    all_gather x1, waiting for transfers between devices, on_device(): lax.all_gather(up_weight, 'fs', axis=0, tiled=True)  103 us
    reduce_scatter x1, waiting for transfers between devices, on_device(): lax.psum_scatter(lax.dot_general(block_rows, down_full, (((1,), (1,)), ((...  42.9 us
    all_gather x1, waiting for transfers between devices, on_device(): full_rows = lax.all_gather(hidden_cols, 'tp', axis=1, tiled=True)  32.4 us
    all_gather x1, waiting for transfers between devices, on_device(): lax.all_gather(value_weight, 'fs', axis=0, tiled=True)  25.1 us
    all_gather x1, waiting for transfers between devices, on_device(): lax.all_gather(gate_weight, 'fs', axis=0, tiled=True)  24.4 us
    dot_general x1, matrix products, on_device(): lax.dot_general(block_rows, down_full, (((1,), (1,)), ((), ())), preferre...  23.6 us
  transfers between devices with their start and end apart: 9, of which 8 were waited for; matrix products, arithmetic and copies ran while one was open for 10% of the time, Pallas kernels for 0%

commit v1 on v0

--- a/solution.py
+++ b/solution.py
@@ -79,7 +79,14 @@
         lax.all_gather(up_weight, "fs", axis=0, tiled=True),
         preferred_element_type=jnp.float32,
     )
-    down_full = lax.all_gather(down_weight, "fs", axis=0, tiled=True)
+    n_dev = lax.axis_size("fs")
+    right = [(i, (i + 1) % n_dev) for i in range(n_dev)]
+    shards = [down_weight]
+    for stride in range(1, n_dev):
+        shards = [lax.ppermute(shards[0], "fs", right), *shards]
+    whole = jnp.concatenate(shards, axis=0)
+    shift = (lax.axis_index("fs") + 1) * shards[-1].shape[0]
+    down_full = jnp.roll(whole, shift, axis=0)
     product = (jax.nn.silu(causal_conv(ffgate, ff_taps.astype(jnp.float32))) * ff_up).astype(
         jnp.bfloat16
     )

time: 586 us -> 531 us (0.906)
  waiting for transfers between devices: 483 us -> 387 us
  starting transfers between devices: 0.31 us -> 24 us
  local copies, waits for them, and re-layouts: 5.05 us -> 20.8 us
    ppermute x0 -> x3, waiting for transfers between devices: none -> 174 us  [on_device(): shards = [lax.ppermute(shards[0], 'fs', right), *shards]]
    all_gather x1 -> x0, waiting for transfers between devices: 115 us -> none  [on_device(): down_full = lax.all_gather(down_weight, 'fs', axis=0, tiled=True)]
    all_gather x1, waiting for transfers between devices: 114 us -> 0.02 us  [on_device(): lax.all_gather(ffgate_weight, 'fs', axis=0, tiled=True)]
    all_gather x1, waiting for transfers between devices: 32.4 us -> 0.01 us  [on_device(): full_rows = lax.all_gather(hidden_cols, 'tp', axis=1, tiled=True)]
    ppermute x0 -> x3, starting transfers between devices: none -> 23.7 us  [on_device(): shards = [lax.ppermute(shards[0], 'fs', right), *shards]]
    unnamed x4 -> x13, local copies, waits for them, and re-layouts: 0.01 us -> 14.5 us
    all_gather x1, waiting for transfers between devices: 103 us -> 95.3 us  [on_device(): lax.all_gather(up_weight, 'fs', axis=0, tiled=True)]
  transfers between devices with their start and end apart: 9 -> 11, of which waited for: 8 -> 8; matrix products, arithmetic and copies ran while one was open for 10% -> 14% of each run, Pallas kernels for 0% -> 0%
where the time goes in v1:
time: 531 us; the launch traced here: 530 us
  waiting for transfers between devices  387 us (73%)
  matrix products  48.8 us (9%)
  other arithmetic  36.1 us (7%)
  starting transfers between devices  24 us (5%)
  local copies, waits for them, and re-layouts  20.8 us (4%)
  between operations  13.7 us (3%)
    ppermute x3, waiting for transfers between devices, on_device(): shards = [lax.ppermute(shards[0], 'fs', right), *shards]  174 us
    all_gather x1, waiting for transfers between devices, on_device(): lax.all_gather(up_weight, 'fs', axis=0, tiled=True)  95.3 us
    reduce_scatter x1, waiting for transfers between devices, on_device(): lax.psum_scatter(lax.dot_general(block_rows, down_full, (((1,), (1,)), ((...  42.9 us
    all_gather x1, waiting for transfers between devices, on_device(): lax.all_gather(value_weight, 'fs', axis=0, tiled=True)  25.1 us
    all_gather x1, waiting for transfers between devices, on_device(): lax.all_gather(gate_weight, 'fs', axis=0, tiled=True)  24.4 us
    dot_general x1, matrix products, on_device(): lax.dot_general(block_rows, down_full, (((1,), (1,)), ((), ())), preferre...  23.7 us
    ppermute x3, starting transfers between devices, on_device(): shards = [lax.ppermute(shards[0], 'fs', right), *shards]  23.7 us
    all_gather x1, waiting for transfers between devices, on_device(): lax.all_gather(head_out, 'tp', axis=1, tiled=True)  22.2 us
  transfers between devices with their start and end apart: 11, of which 8 were waited for; matrix products, arithmetic and copies ran while one was open for 14% of the time, Pallas kernels for 0%

profile of v1, /device:TPU:0, one launch (start us, length us, event | category | flops | bytes accessed | tf_op | source)
XLA Modules:
  0.0 530.4 jit_solution(4765043557034046665)
XLA Ops:
  11.5 3.1 fusion.3
  15.2 24.4 %all-gather.10.cloned.1.call-done = bf16[2048,256]{1,0:T(8,128)(2,1)} async-done(((bf16[512,256]{1,0:T(8,128)(2,1)}), bf16[2048,256]{1,0:T(8,128)(2,1)}) %all-gather.10.cloned.1.call-update) | async-done | bytes 1048592 | tf_op jit(solution)/shard_map/all_gather | solution.py:52
  39.6 3.8 fusion.17
  43.5 25.1 %all-gather.8.cloned.1.call-done = bf16[2048,256]{1,0:T(8,128)(2,1)} async-done(((bf16[512,256]{1,0:T(8,128)(2,1)}), bf16[2048,256]{1,0:T(8,128)(2,1)}) %all-gather.8.cloned.1.call-update) | async-done | bytes 1048592 | tf_op jit(solution)/shard_map/all_gather | solution.py:51
  68.6 3.8 convolution_multiply_fusion
  72.4 4.2 multiply_add_fusion
  78.4 14.4 %multiply_reduce_fusion = f32[1024,2]{1,0:T(8,128)S(1)} fusion(f32[1024,2,128]{2,1,0:T(2,128)S(1)} %reshape.42, f32[1024,2]{1,0:T(8,128)S(1)} %broadcast_multiply_fusion), kind=kLoop, calls=%fused_computation.31 | loop fusion | flops 784384 | bytes 1064960 | tf_op jit(solution)/shard_map/reduce_sum | solution.py:30
  95.4 5.8 %multiply_convert_fusion.1 = bf16[1024,256]{1,0:T(8,128)(2,1)} fusion(f32[128,8,2,128]{3,2,1,0:T(2,128)S(1)} %bitcast.62, f32[128,8,2,128]{3,2,1,0:T(2,128)S(1)} %bitcast.63, f32[256]{0:T(256)S(1)} %convert_element_type.68, f32[1024,256]{1,0:T(8,128)S(1)} %convolution_multiply_fusion, f32[256]{0:T(256)S(1)} %bitcast.87, f32[256]{0:T(256)S(1)} %bitcast.85, ...), kind=kLoop, calls=%fused_computation.30 | loop fusion | flops 18087936 | bytes 3702784 | tf_op jit(solution)/shard_map/convert_element_type | solution.py:60
  101.3 22.2 %all-gather.12.cloned.1.call-done = bf16[1024,1024]{1,0:T(8,128)(2,1)} async-done(((bf16[1024,256]{1,0:T(8,128)(2,1)}), bf16[1024,1024]{1,0:T(8,128)(2,1)}) %all-gather.12.cloned.1.call-update) | async-done | bytes 2097168 | tf_op jit(solution)/shard_map/all_gather | solution.py:63
  123.5 4.4 fusion.14
  130.2 36.8 %collective-permute-done = bf16[512,1536]{1,0:T(8,128)(2,1)S(1)} collective-permute-done((bf16[512,1536]{1,0:T(8,128)(2,1)S(1)}, bf16[512,1536]{1,0:T(8,128)(2,1)S(1)}, u32[]{:S(2)}, u32[]{:S(2)}) %collective-permute-start) | collective-permute-done | bytes 1572896 | tf_op jit(solution)/shard_map/ppermute | solution.py:86
  167.0 66.3 %collective-permute-done.1 = bf16[512,1536]{1,0:T(8,128)(2,1)} collective-permute-done((bf16[512,1536]{1,0:T(8,128)(2,1)S(1)}, bf16[512,1536]{1,0:T(8,128)(2,1)}, u32[]{:S(2)}, u32[]{:S(2)}) %collective-permute-start.1) | collective-permute-done | bytes 1572896 | tf_op jit(solution)/shard_map/ppermute | solution.py:86
  233.3 22.2 %collective-permute-start.2 = (bf16[512,1536]{1,0:T(8,128)(2,1)}, bf16[512,1536]{1,0:T(8,128)(2,1)}, u32[]{:S(2)}, u32[]{:S(2)}) collective-permute-start(bf16[512,1536]{1,0:T(8,128)(2,1)} %collective-permute-done.1), channel_id=1, source_target_pairs={{0,4},{4,8},{8,12},{12,0},{1,5},{5,9},{9,13},{13,1},{2,6},{6,10},{... | collective-permute-start | bytes 4718600 | tf_op jit(solution)/shard_map/ppermute | solution.py:86
  255.5 71.3 %collective-permute-done.2 = bf16[512,1536]{1,0:T(8,128)(2,1)} collective-permute-done((bf16[512,1536]{1,0:T(8,128)(2,1)}, bf16[512,1536]{1,0:T(8,128)(2,1)}, u32[]{:S(2)}, u32[]{:S(2)}) %collective-permute-start.2) | collective-permute-done | bytes 1572896 | tf_op jit(solution)/shard_map/ppermute | solution.py:86
  326.8 2.7 constant_dynamic-update-slice_fusion.7
  329.5 2.7 constant_dynamic-update-slice_fusion.6
  334.7 2.7 constant_dynamic-update-slice_fusion.3
  337.3 2.7 constant_dynamic-update-slice_fusion.2
  342.6 3.1 fusion
  345.7 13.0 %fusion.20 = f32[1024,1536]{1,0:T(8,128)} fusion(bf16[2048,1536]{1,0:T(8,128)(2,1)} %all-gather.18.cloned.1.call-done, bf16[1024,2048]{1,0:T(8,128)(2,1)} %all-gather.16.cloned.1.call-done, f32[2048]{0:T(1024)S(1)} %convert_element_type.73, f32[1024]{0:T(1024)S(1)} %add_rsqrt_fusion.1), kind=kOutput, calls=%fused_computation.25 | convolution fusion | flops 6450839552 | bytes 16789504 | tf_op jit(solution)/shard_map/dot_general | solution.py:72
  358.7 95.3 %all-gather.20.cloned.1.call-done = bf16[2048,1536]{1,0:T(8,128)(2,1)} async-done(((bf16[512,1536]{1,0:T(8,128)(2,1)}), bf16[2048,1536]{1,0:T(8,128)(2,1)}) %all-gather.20.cloned.1.call-update) | async-done | bytes 6291472 | tf_op jit(solution)/shard_map/all_gather | solution.py:79
  454.0 23.7 %fusion.8 = bf16[1024,2048]{1,0:T(8,128)(2,1)} fusion(bf16[4096,1536]{1,0:T(8,128)(2,1)} %constant_dynamic-update-slice_fusion, s32[]{:T(128)S(6)} %select_n.22, f32[1024,1536]{1,0:T(8,128)} %fusion.20, bf16[2048,1536]{1,0:T(8,128)(2,1)} %all-gather.20.cloned.1.call-done, f32[1536]{0:T(1024)S(1)} %get-tuple-element.6, f32[1536]{0:T(1024)S(1)} %get-tuple-element.7, ...), kind=kOutput, calls=%fused_computation.13 | convolution fusion | flops 12912689152 | bytes 27293700 | tf_op jit(solution)/shard_map/dot_general | solution.py:96
  477.8 42.9 %reduce-scatter.2.cloned.1.call-done = bf16[256,2048]{1,0:T(8,128)(2,1)} async-done(((bf16[1024,2048]{1,0:T(8,128)(2,1)}), bf16[256,2048]{1,0:T(8,128)(2,1)}) %reduce-scatter.2.cloned.1.call-update) | async-done | bytes 1048592 | tf_op jit(solution)/shard_map/reduce_scatter | solution.py:95
  520.7 2.9 fusion.24
  (46 shorter events, 17.3 us)
Async XLA Ops:
  6.5 33.1 %all-gather.10.cloned.1.call-start = ((), (), s32[]{:S(2)}) async-start(), calls=%async_computation.2 | async-start | bytes 1310720 | tf_op jit(solution)/shard_map/all_gather | solution.py:52
  7.3 61.3 %all-gather.8.cloned.1.call-start = ((), (), s32[]{:S(2)}) async-start(), calls=%async_computation.1 | async-start | bytes 1310720 | tf_op jit(solution)/shard_map/all_gather | solution.py:51
  8.0 93.3 %all-gather.14.cloned.1.call-start = ((), (), s32[]{:S(2)}) async-start(), calls=%async_computation.4 | async-start | bytes 1310720 | tf_op jit(solution)/shard_map/all_gather | solution.py:53
  8.7 114.8 %all-gather.12.cloned.1.call-start = ((), (), s32[]{:S(2)}) async-start(), calls=%async_computation.3 | async-start | bytes 2621440 | tf_op jit(solution)/shard_map/all_gather | solution.py:63
  101.2 241.4 %all-gather.16.cloned.1.call-start = ((), (), s32[]{:S(2)}) async-start(), calls=%async_computation.5 | async-start | bytes 5242880 | tf_op jit(solution)/shard_map/all_gather | solution.py:69
  101.2 27.3 %copy-start = (bf16[512,1536]{1,0:T(8,128)(2,1)S(1)}, bf16[512,1536]{1,0:T(8,128)(2,1)}, u32[]{:S(2)}) copy-start(bf16[512,1536]{1,0:T(8,128)(2,1)} %param.23) | copy-start | bytes 4718596
  101.3 154.2 %copy-start.2 = (bf16[2048]{0:T(1024)(128)(2,1)S(1)}, bf16[2048]{0:T(1024)(128)(2,1)}, u32[]{:S(2)}) copy-start(bf16[2048]{0:T(1024)(128)(2,1)} %param.19) | copy-start | bytes 12292
  101.3 154.2 %copy-start.1 = (bf16[3,1536]{1,0:T(4,128)(2,1)S(1)}, bf16[3,1536]{1,0:T(4,128)(2,1)}, u32[]{:S(2)}) copy-start(bf16[3,1536]{1,0:T(4,128)(2,1)} %param.22) | copy-start | bytes 27652
  127.9 217.8 %all-gather.18.cloned.1.call-start = ((), (), s32[]{:S(2)}) async-start(), calls=%async_computation.6 | async-start | bytes 7864320 | tf_op jit(solution)/shard_map/all_gather | solution.py:74
  128.5 325.5 %all-gather.20.cloned.1.call-start = ((), (), s32[]{:S(2)}) async-start(), calls=%async_computation.7 | async-start | bytes 7864320 | tf_op jit(solution)/shard_map/all_gather | solution.py:79
  128.6 38.4 %collective-permute-start = (bf16[512,1536]{1,0:T(8,128)(2,1)S(1)}, bf16[512,1536]{1,0:T(8,128)(2,1)S(1)}, u32[]{:S(2)}, u32[]{:S(2)}) collective-permute-start(bf16[512,1536]{1,0:T(8,128)(2,1)S(1)} %copy-done), channel_id=1, source_target_pairs={{0,4},{4,8},{8,12},{12,0},{1,5},{5,9},{9,13},{13,1},{2,6},{6,10},{... | collective-permute-start | bytes 4718600 | tf_op jit(solution)/shard_map/ppermute | solution.py:86
  130.1 390.5 %reduce-scatter.2.cloned.1.call-start = ((), (), s32[]{:S(2)}) async-start(), calls=%async_computation.8 | async-start | bytes 5242880 | tf_op jit(solution)/shard_map/reduce_scatter | solution.py:95
  167.0 66.3 %collective-permute-start.1 = (bf16[512,1536]{1,0:T(8,128)(2,1)S(1)}, bf16[512,1536]{1,0:T(8,128)(2,1)}, u32[]{:S(2)}, u32[]{:S(2)}) collective-permute-start(bf16[512,1536]{1,0:T(8,128)(2,1)S(1)} %collective-permute-done), channel_id=1, source_target_pairs={{0,4},{4,8},{8,12},{12,0},{1,5},{5,9},{9,13},{13,1},{2,6},{6,10},{... | collective-permute-start | bytes 4718600 | tf_op jit(solution)/shard_map/ppermute | solution.py:86
  233.3 93.6 %collective-permute-start.2 = (bf16[512,1536]{1,0:T(8,128)(2,1)}, bf16[512,1536]{1,0:T(8,128)(2,1)}, u32[]{:S(2)}, u32[]{:S(2)}) collective-permute-start(bf16[512,1536]{1,0:T(8,128)(2,1)} %collective-permute-done.1), channel_id=1, source_target_pairs={{0,4},{4,8},{8,12},{12,0},{1,5},{5,9},{9,13},{13,1},{2,6},{6,10},{... | collective-permute-start | bytes 4718600 | tf_op jit(solution)/shard_map/ppermute | solution.py:86
Sparse Core Ops, SparseCore 0:
  8.9 30.6 all-gather.9
  41.2 27.3 all-gather.7
  70.2 27.3 all-gather.13
  101.3 22.1 all-gather.11
  128.1 34.4 all-gather.15
  164.0 175.7 all-gather.17
  341.4 112.5 all-gather.19
  477.9 42.7 reduce-scatter.1
